TPU v7x, 256 devices: a whole 4x4x8 slice. The times are simulated.
256 devices in a mesh: kv: 32 (over z, y), tp: 8 (over x, core).
Axes of the slice: x: 4, y: 4, z: 8, core: 2. Of those that a mesh axis runs over, the one named last changes fastest.
Arguments:
- tokens: bfloat16 [64, 4096], P(None, ('kv', 'tp')), may hold values from -8 to 8
- gate_weights: bfloat16 [2, 4096, 11264], P(None, None, ('kv', 'tp')), may hold values from -0.09375 to 0.09375
- up_weights: bfloat16 [2, 4096, 11264], P(None, None, ('kv', 'tp')), may hold values from -0.09375 to 0.09375
- down_weights: bfloat16 [2, 11264, 4096], P(None, ('kv', 'tp')), may hold values from -1 to 1
- norm_gain: bfloat16 [3, 4096], P(None, ('kv', 'tp')), may hold values from 0.25 to 4.5
- norm_bias: bfloat16 [3, 4096], P(None, ('kv', 'tp')), may hold values from -3 to 3
- query_weight: bfloat16 [4096, 4096], P('kv', 'tp'), may hold values from -0.09375 to 0.09375
- forget_weight: bfloat16 [4096, 4096], P('kv', 'tp'), may hold values from -0.09375 to 0.09375
- input_weight: bfloat16 [4096, 4096], P('kv', 'tp'), may hold values from -0.09375 to 0.09375
- outgate_weight: bfloat16 [4096, 4096], P('kv', 'tp'), may hold values from -0.09375 to 0.09375
- lower_bound: float32 [4096], P('tp'), may hold values from 0.05 to 0.9
- head_gain: float32 [4096], P('tp'), may hold values from 0.1 to 1.9
- out_weight: bfloat16 [4096, 4096], P('tp'), may hold values from -0.25 to 0.25
- state: float32 [64, 32, 128, 128], P('kv', 'tp'), may hold values from -3 to 3
Outputs:
- mixed: bfloat16 [64, 4096], P(None, ('kv', 'tp'))
- new_state: float32 [64, 32, 128, 128], P('kv', 'tp')
All inputs are finite; a program needn't handle non-finite values.
Results may differ from a plain program's by a relative error of at most 0.022.
Values may be sent and summed in bfloat16 or wider, within the bound.
No kernel may reach another device: no remote copies, remote signals or barrier semaphores. Data moves between devices by JAX's collectives and lax.ppermute only.
A program may use at most 64 MiB of HBM per device.

v0:
```python
import jax
import jax.numpy as jnp
from jax import lax
from jax.sharding import Mesh
from jax.sharding import PartitionSpec as P

HEAD = 128
KV_TP = ("kv_0", "kv_1", "tp_0", "tp_1")
KV = ("kv_0", "kv_1")
TP = ("tp_0", "tp_1")
residual_scale = 8.0**0.25
norm_eps = 1e-05
head_eps = 1e-06


def turned_gather(arrays, axis, dims):
    turned = [jnp.moveaxis(a, dim, 0) for a, dim in zip(arrays, dims)]
    both = jnp.concatenate([t.reshape(len(t), -1) for t in turned], axis=1)
    whole, at, gathered = (lax.all_gather(both, axis, axis=0, tiled=True), 0, [])
    for t, dim in zip(turned, dims):
        section = whole[:, at : at + t[0].size].reshape(-1, *t.shape[1:])
        gathered.append(jnp.moveaxis(section, 0, dim))
        at += t[0].size
    return tuple(gathered)


def rows_for(lines, count):
    spare = -lines.shape[0] % count
    if not spare:
        return lines
    return jnp.concatenate([lines, jnp.zeros((spare, *lines.shape[1:]), lines.dtype)])


def from_everyone(x, axis):
    copies = jnp.broadcast_to(x, (lax.axis_size(axis), *x.shape))
    return lax.all_to_all(copies, axis, split_axis=0, concat_axis=0, tiled=True)


def laid_out(blocks, dim):
    blocks = jnp.moveaxis(blocks, 0, dim)
    shape = blocks.shape
    return blocks.reshape(*shape[:dim], shape[dim] * shape[dim + 1], *shape[dim + 2 :])


def whole_of(x, axes, dim):
    far, near = axes
    leading = from_everyone(x, far)
    blocks = jnp.swapaxes(from_everyone(leading, near), 0, 1)
    return laid_out(blocks.reshape(-1, *x.shape), dim)


def in_blocks(x, dim, count):
    before, after = (x.shape[:dim], x.shape[dim + 1 :])
    return jnp.moveaxis(x.reshape(*before, count, -1, *after), dim, 0)


def sum_at_owner(x, axis, dim):
    blocks = in_blocks(x, dim, lax.axis_size(axis))
    arrived = lax.all_to_all(blocks, axis, split_axis=0, concat_axis=0, tiled=True)
    return arrived.sum(axis=0)


def sum_by_axis(x, axes, dim):
    far, near = axes
    blocks = in_blocks(x, dim, lax.axis_size(far))
    nearer = sum_at_owner(blocks, near, dim + 1)
    arrived = lax.all_to_all(nearer, far, split_axis=0, concat_axis=0, tiled=True)
    return arrived.sum(axis=0)


def nested_sum(x, axes):
    lines = x.reshape(-1)
    padded = rows_for(lines, lax.axis_size(axes[0]) * lax.axis_size(axes[1]))
    whole = whole_of(sum_by_axis(padded, axes, 0), axes, 0)
    return lax.slice_in_dim(whole, 0, len(lines)).reshape(x.shape)


def sum_at_owner_2(x, axis, dim):
    blocks = in_blocks(x, dim, lax.axis_size(axis))
    arrived = lax.all_to_all(blocks, axis, split_axis=0, concat_axis=0, tiled=True)
    return arrived.astype(jnp.float32).sum(axis=0)


def gathered_copies(x, axis, dim):
    blocks = from_everyone(x, axis)
    return laid_out(blocks, dim)


def whole_norm(stream, gain_row, bias_row):
    row_mean = jnp.mean(stream, axis=-1, keepdims=True)
    centred = stream - row_mean
    spread = jnp.mean(centred * centred, axis=-1, keepdims=True)
    return centred * lax.rsqrt(spread + norm_eps) * gain_row.astype(jnp.float32) + bias_row.astype(
        jnp.float32
    )


def ffn_partial(whole_rows, gate_w, up_w, down_w):
    gate_proj = jnp.dot(whole_rows, gate_w, preferred_element_type=jnp.float32)
    up_proj = jnp.dot(whole_rows, up_w, preferred_element_type=jnp.float32)
    hidden = (jax.nn.silu(gate_proj) * up_proj).astype(jnp.bfloat16)
    return jnp.dot(hidden, down_w, preferred_element_type=jnp.float32)


def local(
    tokens,
    gate_weights,
    up_weights,
    down_weights,
    norm_gain,
    norm_bias,
    query_weight,
    forget_weight,
    input_weight,
    outgate_weight,
    lower_bound,
    head_gain,
    out_weight,
    state,
):
    own_cols = tokens.shape[1]
    col_offset = lax.axis_index(KV_TP) * own_cols
    whole_tokens, whole_gain, whole_bias = turned_gather(
        (tokens, norm_gain, norm_bias), KV_TP, (1, 1, 1)
    )

    def finish(partial_value, residual_whole, index, want_whole):
        total = nested_sum(partial_value, (("kv_0", "kv_1"), ("tp_0", "tp_1")))
        stream = residual_scale * residual_whole + 0.5 * total
        normed = whole_norm(stream, whole_gain[index], whole_bias[index]).astype(jnp.bfloat16)
        if want_whole:
            return normed
        return lax.dynamic_slice_in_dim(normed, col_offset, own_cols, 1)

    partial_one = ffn_partial(whole_tokens, gate_weights[0], up_weights[0], down_weights[0])
    normed_one = finish(partial_one, whole_tokens.astype(jnp.float32), 0, True)
    seq_count = state.shape[0]
    head_count = state.shape[1]
    head_cols = query_weight.shape[1]
    weight_rows = query_weight.shape[0]
    seq_offset = lax.axis_index(KV) * seq_count
    block_rows = lax.dynamic_slice_in_dim(
        normed_one, lax.axis_index(KV) * weight_rows, weight_rows, 1
    )
    weights = (query_weight, forget_weight, input_weight, outgate_weight)
    projected = sum_at_owner_2(
        jnp.concatenate(
            [jnp.dot(block_rows, weight, preferred_element_type=jnp.float32) for weight in weights],
            axis=1,
        ).astype(jnp.bfloat16),
        KV,
        0,
    ).astype(jnp.bfloat16)
    query_pre = projected[:, :head_cols].astype(jnp.float32).reshape(seq_count, head_count, HEAD)
    forget_pre = (
        projected[:, head_cols : 2 * head_cols]
        .astype(jnp.float32)
        .reshape(seq_count, head_count, HEAD)
    )
    input_pre = (
        projected[:, 2 * head_cols : 3 * head_cols]
        .astype(jnp.float32)
        .reshape(seq_count, head_count, HEAD)
    )
    outgate_pre = projected[:, 3 * head_cols :].astype(jnp.float32)
    low_bound = lower_bound.reshape(head_count, HEAD)
    forget = low_bound + (1.0 - low_bound) * jax.nn.sigmoid(forget_pre)
    key_part = (1.0 - low_bound) * jax.nn.sigmoid(-forget_pre)
    updated = forget[..., None] * state + key_part[..., None] * input_pre[:, :, None, :]
    readout = jnp.einsum(
        "shd,shde->she", jax.nn.silu(query_pre), updated, precision=lax.Precision.HIGHEST
    )
    readout = readout * lax.rsqrt(jnp.mean(readout * readout, axis=-1, keepdims=True) + head_eps)
    gated_out = (
        readout.reshape(seq_count, head_cols) * head_gain * jax.nn.silu(outgate_pre)
    ).astype(jnp.bfloat16)
    mixer_part = jnp.dot(gated_out, out_weight, preferred_element_type=jnp.float32)
    head_sum = sum_at_owner_2(mixer_part.astype(jnp.bfloat16), TP, 1)
    piece_cols = head_sum.shape[1]
    own_normed = lax.dynamic_slice_in_dim(normed_one, seq_offset, seq_count, 0)
    own_normed = lax.dynamic_slice_in_dim(
        own_normed, lax.axis_index(TP) * piece_cols, piece_cols, 1
    )
    stream_own = (residual_scale * own_normed.astype(jnp.float32) + head_sum).astype(jnp.bfloat16)
    seq_rows = gathered_copies(stream_own, TP, 1)
    stream_two = gathered_copies(seq_rows, KV, 0)
    normed_two = whole_norm(stream_two.astype(jnp.float32), whole_gain[1], whole_bias[1]).astype(
        jnp.bfloat16
    )
    partial_two = ffn_partial(normed_two, gate_weights[1], up_weights[1], down_weights[1])
    mixed = finish(partial_two, normed_two.astype(jnp.float32), 2, False)
    return (mixed, updated)


def solution(mesh):
    finer = Mesh(mesh.devices.reshape(8, 4, 4, 2), ("kv_0", "kv_1", "tp_0", "tp_1"))
    in_specs = (
        P(None, KV_TP),
        P(None, None, KV_TP),
        P(None, None, KV_TP),
        P(None, KV_TP, None),
        P(None, KV_TP),
        P(None, KV_TP),
        P(KV, TP),
        P(KV, TP),
        P(KV, TP),
        P(KV, TP),
        P(TP),
        P(TP),
        P(TP, None),
        P(KV, TP, None, None),
    )
    out_specs = (P(None, KV_TP), P(KV, TP, None, None))
    return jax.shard_map(local, mesh=finer, in_specs=in_specs, out_specs=out_specs, check_vma=False)
```

profile of v0, /device:TPU:1, one launch (start us, length us, event | category | flops | bytes accessed | tf_op | source)
XLA Modules:
  0.0 302.1 jit_solution(11334063490553480618)
XLA Ops:
  3.0 67.7 %all_gather.3 = bf16[4096,70]{1,0:T(8,128)(2,1)S(1)} all-gather(bf16[16,70]{1,0:T(8,128)(2,1)S(1)} %pad_maximum_fusion.1), channel_id=1, replica_groups=mesh['kv_0'=8,'kv_1'=4,'tp_0'=4,'tp_1'=2] {'kv_0','kv_1','tp_0','tp_1'}, dimensions={0}, use_global_device_ids=true | all-gather | bytes 575680 | tf_op jit(solution)/shard_map/all_gather | solution.py:19
  70.8 4.6 %fusion.54 = (bf16[1,44,4096]{2,0,1:T(2,128)(2,1)}, bf16[1,44,4096]{2,0,1:T(2,128)(2,1)}) fusion(bf16[2,44,4096]{2,0,1:T(2,128)(2,1)} %param.17), kind=kLoop, calls=%fused_computation.115 | loop fusion | bytes 1441792 | tf_op jit(solution)/shard_map/slice | solution.py:190
  75.3 2.8 fusion.53
  83.7 18.4 %all_to_all.76 = f32[8,32,1024]{2,1,0:T(8,128)S(1)} all-to-all(f32[8,32,1024]{2,1,0:T(8,128)S(1)} %bitcast.90), channel_id=1, replica_groups=mesh['kv_0'=8,'kv_1'=4,'tp_0'=4,'tp_1'=2] {'tp_0','tp_1'}, dimensions={0} | all-to-all | bytes 2097152 | tf_op jit(solution)/shard_map/all_to_all | solution.py:59
  102.2 14.2 %all_to_all.77 = f32[32,1,1024]{2,1,0:T(1,128)S(1)} all-to-all(f32[32,1,1024]{2,1,0:T(1,128)S(1)} %all_to_all.49), channel_id=1, replica_groups=mesh['kv_0'=8,'kv_1'=4,'tp_0'=4,'tp_1'=2] {'kv_0','kv_1'}, dimensions={0} | all-to-all | bytes 262144 | tf_op jit(solution)/shard_map/all_to_all | solution.py:67
  117.3 3.9 %all-to-all-start.2 = ((f32[32,1,1024]{2,1,0:T(1,128)}), f32[32,1,1024]{2,1,0:T(1,128)S(1)}, u32[]{:S(2)}, u32[]{:S(2)}) async-start(f32[32,1,1024]{2,1,0:T(1,128)} %broadcast_in_dim.12), calls=%async_computation.2 | async-start | bytes 262144 | tf_op jit(solution)/shard_map/all_to_all | solution.py:36
  121.5 9.1 %all-to-all-done.2 = f32[32,1,1024]{2,1,0:T(1,128)S(1)} async-done(((f32[32,1,1024]{2,1,0:T(1,128)}), f32[32,1,1024]{2,1,0:T(1,128)S(1)}, u32[]{:S(2)}, u32[]{:S(2)}) %all-to-all-start.2) | async-done | bytes 131104 | tf_op jit(solution)/shard_map/all_to_all | solution.py:36
  131.7 7.1 %all-to-all-start.3 = ((f32[8,32,1024]{2,1,0:T(8,128)}), f32[8,32,1024]{2,1,0:T(8,128)S(1)}, u32[]{:S(2)}, u32[]{:S(2)}) async-start(f32[8,32,1024]{2,1,0:T(8,128)} %broadcast_in_dim.13), calls=%async_computation.3 | async-start | bytes 2097152 | tf_op jit(solution)/shard_map/all_to_all | solution.py:36
  139.5 3.4 %convert_reduce_fusion = (f32[4096]{0:T(1024)S(1)}, f32[4096]{0:T(1024)S(1)}, f32[4096]{0:T(1024)S(1)}, f32[4096]{0:T(1024)S(1)}, f32[4096]{0:T(1024)S(1)}, /*index=5*/f32[4096]{0:T(1024)S(1)}) fusion(bf16[3,4096]{0,1:T(8,128)(2,1)S(1)} %get-tuple-element.13, bf16[3,4096]{0,1:T(8,128)(2,1)S(1)} %get-tuple-element.12), kind=kLoop, calls=%fused_computation.1 | loop fusion | flops 24576 | bytes 147456 | tf_op jit(solution)/shard_map/add | solution.py:93
  142.8 11.0 %all-to-all-done.3 = f32[8,32,1024]{2,1,0:T(8,128)S(1)} async-done(((f32[8,32,1024]{2,1,0:T(8,128)}), f32[8,32,1024]{2,1,0:T(8,128)S(1)}, u32[]{:S(2)}, u32[]{:S(2)}) %all-to-all-start.3) | async-done | bytes 1048608 | tf_op jit(solution)/shard_map/all_to_all | solution.py:36
  157.7 3.9 %all-to-all-start.4 = ((bf16[32,2,2048]{2,1,0:T(2,128)(2,1)}), bf16[32,2,2048]{2,1,0:T(2,128)(2,1)S(1)}, u32[]{:S(2)}, u32[]{:S(2)}) async-start(bf16[32,2,2048]{2,1,0:T(2,128)(2,1)} %pad_maximum_fusion), calls=%async_computation.4 | async-start | bytes 524288 | tf_op jit(solution)/shard_map/all_to_all | solution.py:80
  161.6 11.4 %all-to-all-done.4 = bf16[32,2,2048]{2,1,0:T(2,128)(2,1)S(1)} async-done(((bf16[32,2,2048]{2,1,0:T(2,128)(2,1)}), bf16[32,2,2048]{2,1,0:T(2,128)(2,1)S(1)}, u32[]{:S(2)}, u32[]{:S(2)}) %all-to-all-start.4) | async-done | bytes 262176 | tf_op jit(solution)/shard_map/all_to_all | solution.py:80
  175.2 3.5 %convolution_convert_fusion = bf16[2,4096]{1,0:T(2,128)(2,1)} fusion(bf16[512,4096]{1,0:T(8,128)(2,1)} %param.26, f32[1,2,4,128]{3,2,1,0:T(4,128)S(1)} %multiply_bitcast_fusion.2, bf16[2,2048]{1,0:T(2,128)(2,1)S(1)} %reduce_sum.124, f32[512]{0:T(512)S(1)} %copy-done.12), kind=kOutput, calls=%fused_computation | convolution fusion | flops 8404992 | bytes 4218880 | tf_op jit(solution)/shard_map/dot_general | solution.py:177
  178.7 5.9 %all-to-all-start.5 = ((bf16[8,2,512]{2,1,0:T(2,128)(2,1)}), bf16[8,2,512]{2,1,0:T(2,128)(2,1)S(1)}, u32[]{:S(2)}, u32[]{:S(2)}) async-start(bf16[8,2,512]{2,1,0:T(2,128)(2,1)} %bitcast.17), calls=%async_computation.5 | async-start | bytes 32768 | tf_op jit(solution)/shard_map/all_to_all | solution.py:80
  184.6 4.7 %all-to-all-done.5 = bf16[8,2,512]{2,1,0:T(2,128)(2,1)S(1)} async-done(((bf16[8,2,512]{2,1,0:T(2,128)(2,1)}), bf16[8,2,512]{2,1,0:T(2,128)(2,1)S(1)}, u32[]{:S(2)}, u32[]{:S(2)}) %all-to-all-start.5) | async-done | bytes 16416 | tf_op jit(solution)/shard_map/all_to_all | solution.py:80
  189.4 7.7 %all_to_all.78 = bf16[8,2,512]{2,1,0:T(2,128)(2,1)S(1)} all-to-all(bf16[8,2,512]{2,1,0:T(2,128)(2,1)S(1)} %broadcast_in_dim.14), channel_id=1, replica_groups=mesh['kv_0'=8,'kv_1'=4,'tp_0'=4,'tp_1'=2] {'tp_0','tp_1'}, dimensions={0} | all-to-all | bytes 32768 | tf_op jit(solution)/shard_map/all_to_all | solution.py:36
  197.6 19.6 %all_to_all.79 = bf16[32,2,4096]{2,1,0:T(2,128)(2,1)S(1)} all-to-all(bf16[32,2,4096]{2,1,0:T(2,128)(2,1)S(1)} %broadcast_in_dim.15), channel_id=1, replica_groups=mesh['kv_0'=8,'kv_1'=4,'tp_0'=4,'tp_1'=2] {'kv_0','kv_1'}, dimensions={0} | all-to-all | bytes 1048576 | tf_op jit(solution)/shard_map/all_to_all | solution.py:36
  220.2 2.2 fusion.3
  223.4 19.7 %all_to_all.80 = f32[8,32,1024]{2,1,0:T(8,128)S(1)} all-to-all(f32[8,32,1024]{2,1,0:T(8,128)S(1)} %bitcast.91), channel_id=1, replica_groups=mesh['kv_0'=8,'kv_1'=4,'tp_0'=4,'tp_1'=2] {'tp_0','tp_1'}, dimensions={0} | all-to-all | bytes 2097152 | tf_op jit(solution)/shard_map/all_to_all | solution.py:59
  243.3 13.5 %all_to_all.81 = f32[32,1,1024]{2,1,0:T(1,128)S(1)} all-to-all(f32[32,1,1024]{2,1,0:T(1,128)S(1)} %all_to_all.59), channel_id=1, replica_groups=mesh['kv_0'=8,'kv_1'=4,'tp_0'=4,'tp_1'=2] {'kv_0','kv_1'}, dimensions={0} | all-to-all | bytes 262144 | tf_op jit(solution)/shard_map/all_to_all | solution.py:67
  257.6 3.9 %all-to-all-start.10 = ((f32[32,1,1024]{2,1,0:T(1,128)}), f32[32,1,1024]{2,1,0:T(1,128)S(1)}, u32[]{:S(2)}, u32[]{:S(2)}) async-start(f32[32,1,1024]{2,1,0:T(1,128)} %broadcast_in_dim.16), calls=%async_computation.10 | async-start | bytes 262144 | tf_op jit(solution)/shard_map/all_to_all | solution.py:36
  262.0 8.9 %all-to-all-done.10 = f32[32,1,1024]{2,1,0:T(1,128)S(1)} async-done(((f32[32,1,1024]{2,1,0:T(1,128)}), f32[32,1,1024]{2,1,0:T(1,128)S(1)}, u32[]{:S(2)}, u32[]{:S(2)}) %all-to-all-start.10) | async-done | bytes 131104 | tf_op jit(solution)/shard_map/all_to_all | solution.py:36
  272.1 7.1 %all-to-all-start.11 = ((f32[8,32,1024]{2,1,0:T(8,128)}), f32[8,32,1024]{2,1,0:T(8,128)S(1)}, u32[]{:S(2)}, u32[]{:S(2)}) async-start(f32[8,32,1024]{2,1,0:T(8,128)} %broadcast_in_dim.17), calls=%async_computation.11 | async-start | bytes 2097152 | tf_op jit(solution)/shard_map/all_to_all | solution.py:36
  280.4 13.8 %all-to-all-done.11 = f32[8,32,1024]{2,1,0:T(8,128)S(1)} async-done(((f32[8,32,1024]{2,1,0:T(8,128)}), f32[8,32,1024]{2,1,0:T(8,128)S(1)}, u32[]{:S(2)}, u32[]{:S(2)}) %all-to-all-start.11) | async-done | bytes 1048608 | tf_op jit(solution)/shard_map/all_to_all | solution.py:36
  (113 shorter events, 33.2 us)
Async XLA Ops:
  0.6 155.3 %copy-start = (bf16[128,512]{1,0:T(8,128)(2,1)S(1)}, bf16[128,512]{1,0:T(8,128)(2,1)}, u32[]{:S(2)}) copy-start(bf16[128,512]{1,0:T(8,128)(2,1)} %param.23) | copy-start | bytes 393220
  0.6 74.7 %copy-start.1 = (bf16[2,4096,44]{1,0,2:T(2,128)(2,1)S(1)}, bf16[2,4096,44]{1,0,2:T(2,128)(2,1)}, u32[]{:S(2)}) copy-start(bf16[2,4096,44]{1,0,2:T(2,128)(2,1)} %param.16) | copy-start | bytes 2162692
  75.3 2.8 copy-start.2
  78.1 2.4 copy-start.6
  117.3 13.3 %all-to-all-start.2 = ((f32[32,1,1024]{2,1,0:T(1,128)}), f32[32,1,1024]{2,1,0:T(1,128)S(1)}, u32[]{:S(2)}, u32[]{:S(2)}) async-start(f32[32,1,1024]{2,1,0:T(1,128)} %broadcast_in_dim.12), calls=%async_computation.2 | async-start | bytes 262144 | tf_op jit(solution)/shard_map/all_to_all | solution.py:36
  131.7 22.1 %all-to-all-start.3 = ((f32[8,32,1024]{2,1,0:T(8,128)}), f32[8,32,1024]{2,1,0:T(8,128)S(1)}, u32[]{:S(2)}, u32[]{:S(2)}) async-start(f32[8,32,1024]{2,1,0:T(8,128)} %broadcast_in_dim.13), calls=%async_computation.3 | async-start | bytes 2097152 | tf_op jit(solution)/shard_map/all_to_all | solution.py:36
  155.3 0.9 copy-start.8
  155.3 1.1 copy-start.9
  155.3 1.3 copy-start.10
  155.6 6.0 %copy-start.11 = (f32[512]{0:T(512)S(1)}, f32[512]{0:T(512)}, u32[]{:S(2)}) copy-start(f32[512]{0:T(512)} %param.24) | copy-start | bytes 6148
  155.6 17.7 %copy-start.7 = (f32[2,4,128,128]{3,2,1,0:T(8,128)S(1)}, f32[2,4,128,128]{3,2,1,0:T(8,128)}, u32[]{:S(2)}) copy-start(f32[2,4,128,128]{3,2,1,0:T(8,128)} %param.27) | copy-start | bytes 1572868
  156.1 19.1 %copy-start.12 = (f32[512]{0:T(512)S(1)}, f32[512]{0:T(512)}, u32[]{:S(2)}) copy-start(f32[512]{0:T(512)} %param.25) | copy-start | bytes 6148
  157.7 15.3 %all-to-all-start.4 = ((bf16[32,2,2048]{2,1,0:T(2,128)(2,1)}), bf16[32,2,2048]{2,1,0:T(2,128)(2,1)S(1)}, u32[]{:S(2)}, u32[]{:S(2)}) async-start(bf16[32,2,2048]{2,1,0:T(2,128)(2,1)} %pad_maximum_fusion), calls=%async_computation.4 | async-start | bytes 524288 | tf_op jit(solution)/shard_map/all_to_all | solution.py:80
  173.7 0.8 copy-start.3
  178.7 10.6 %all-to-all-start.5 = ((bf16[8,2,512]{2,1,0:T(2,128)(2,1)}), bf16[8,2,512]{2,1,0:T(2,128)(2,1)S(1)}, u32[]{:S(2)}, u32[]{:S(2)}) async-start(bf16[8,2,512]{2,1,0:T(2,128)(2,1)} %bitcast.17), calls=%async_computation.5 | async-start | bytes 32768 | tf_op jit(solution)/shard_map/all_to_all | solution.py:80
  197.6 22.1 %copy-start.5 = (bf16[1,4096,44]{1,0,2:T(2,128)(2,1)S(1)}, bf16[1,4096,44]{1,0,2:T(2,128)(2,1)}, u32[]{:S(2)}) copy-start(bf16[1,4096,44]{1,0,2:T(2,128)(2,1)} %get-tuple-element.14) | copy-start | bytes 1081348
  217.2 3.1 %copy-start.4 = (bf16[1,44,4096]{2,0,1:T(2,128)(2,1)S(1)}, bf16[1,44,4096]{2,0,1:T(2,128)(2,1)}, u32[]{:S(2)}) copy-start(bf16[1,44,4096]{2,0,1:T(2,128)(2,1)} %get-tuple-element.18) | copy-start | bytes 1081348
  257.6 13.3 %all-to-all-start.10 = ((f32[32,1,1024]{2,1,0:T(1,128)}), f32[32,1,1024]{2,1,0:T(1,128)S(1)}, u32[]{:S(2)}, u32[]{:S(2)}) async-start(f32[32,1,1024]{2,1,0:T(1,128)} %broadcast_in_dim.16), calls=%async_computation.10 | async-start | bytes 262144 | tf_op jit(solution)/shard_map/all_to_all | solution.py:36
  272.1 22.1 %all-to-all-start.11 = ((f32[8,32,1024]{2,1,0:T(8,128)}), f32[8,32,1024]{2,1,0:T(8,128)S(1)}, u32[]{:S(2)}, u32[]{:S(2)}) async-start(f32[8,32,1024]{2,1,0:T(8,128)} %broadcast_in_dim.17), calls=%async_computation.11 | async-start | bytes 2097152 | tf_op jit(solution)/shard_map/all_to_all | solution.py:36
where the time goes:
time: 303 us; the launch traced here: 302 us
  blocking collectives  161 us (53%)
  waiting for transfers between devices  58.8 us (19%)
  starting transfers between devices  31.7 us (10%)
  local copies, waits for them, and re-layouts  24.7 us (8%)
  other arithmetic  14.9 us (5%)
  matrix products  10 us (3%)
    all_gather x1, blocking collectives, turned_gather(): lax.all_gather(both, axis, axis=0, tiled=True)  67.7 us
    all_to_all x4, waiting for transfers between devices, from_everyone(): return lax.all_to_all(copies, axis, split_axis=0, concat_axis=0, tiled=True)  42.7 us
    all_to_all x2, blocking collectives, sum_at_owner(): lax.all_to_all(blocks, axis, split_axis=0, concat_axis=0, tiled=True)  38.1 us
    all_to_all x2, blocking collectives, sum_by_axis(): lax.all_to_all(nearer, far, split_axis=0, concat_axis=0, tiled=True)  27.8 us
    all_to_all x2, blocking collectives, from_everyone(): return lax.all_to_all(copies, axis, split_axis=0, concat_axis=0, tiled=True)  27.3 us
    all_to_all x4, starting transfers between devices, from_everyone(): return lax.all_to_all(copies, axis, split_axis=0, concat_axis=0, tiled=True)  22 us
    all_to_all x2, waiting for transfers between devices, sum_at_owner_2(): lax.all_to_all(blocks, axis, split_axis=0, concat_axis=0, tiled=True)  16.1 us
    all_to_all x2, starting transfers between devices, sum_at_owner_2(): lax.all_to_all(blocks, axis, split_axis=0, concat_axis=0, tiled=True)  9.75 us
  transfers between devices with their start and end apart: 6, of which 6 were waited for; matrix products, arithmetic and copies ran while one was open for 2% of the time, Pallas kernels for 0%

commit v1 on v0

--- a/solution.py
+++ b/solution.py
@@ -13,10 +13,17 @@
 head_eps = 1e-06
 
 
+def gather_over(x, axis, d):
+    size = lax.axis_size(axis)
+    blocks = jnp.stack([x for _ in range(size)])
+    blocks = lax.all_to_all(blocks, axis, split_axis=0, concat_axis=0)
+    return jnp.concatenate(blocks, axis=d)
+
+
 def turned_gather(arrays, axis, dims):
     turned = [jnp.moveaxis(a, dim, 0) for a, dim in zip(arrays, dims)]
     both = jnp.concatenate([t.reshape(len(t), -1) for t in turned], axis=1)
-    whole, at, gathered = (lax.all_gather(both, axis, axis=0, tiled=True), 0, [])
+    whole, at, gathered = (gather_over(both, axis, 0), 0, [])
     for t, dim in zip(turned, dims):
         section = whole[:, at : at + t[0].size].reshape(-1, *t.shape[1:])
         gathered.append(jnp.moveaxis(section, 0, dim))

time: 303 us -> 273 us (0.901)
  blocking collectives: 161 us -> 93 us
  waiting for transfers between devices: 58.8 us -> 81.2 us
  starting transfers between devices: 31.7 us -> 47.3 us
    all_gather x1 -> x0, blocking collectives: 67.7 us -> none  [turned_gather(): lax.all_gather(both, axis, axis=0, tiled=True)]
    all_to_all x0 -> x1, waiting for transfers between devices: none -> 22.4 us  [gather_over(): blocks = lax.all_to_all(blocks, axis, split_axis=0, concat_axis=0)]
    all_to_all x0 -> x1, starting transfers between devices: none -> 15.6 us  [gather_over(): blocks = lax.all_to_all(blocks, axis, split_axis=0, concat_axis=0)]
  transfers between devices with their start and end apart: 6 -> 7, of which waited for: 6 -> 7; matrix products, arithmetic and copies ran while one was open for 2% -> 5% of each run, Pallas kernels for 0% -> 0%
where the time goes in v1:
time: 273 us; the launch traced here: 272 us
  blocking collectives  93 us (34%)
  waiting for transfers between devices  81.2 us (30%)
  starting transfers between devices  47.3 us (17%)
  local copies, waits for them, and re-layouts  24.7 us (9%)
  other arithmetic  14.8 us (5%)
  matrix products  10.2 us (4%)
    all_to_all x4, waiting for transfers between devices, from_everyone(): return lax.all_to_all(copies, axis, split_axis=0, concat_axis=0, tiled=True)  42.7 us
    all_to_all x2, blocking collectives, sum_at_owner(): lax.all_to_all(blocks, axis, split_axis=0, concat_axis=0, tiled=True)  39.7 us
    all_to_all x2, blocking collectives, from_everyone(): return lax.all_to_all(copies, axis, split_axis=0, concat_axis=0, tiled=True)  27.3 us
    all_to_all x2, blocking collectives, sum_by_axis(): lax.all_to_all(nearer, far, split_axis=0, concat_axis=0, tiled=True)  26 us
    all_to_all x1, waiting for transfers between devices, gather_over(): blocks = lax.all_to_all(blocks, axis, split_axis=0, concat_axis=0)  22.4 us
    all_to_all x4, starting transfers between devices, from_everyone(): return lax.all_to_all(copies, axis, split_axis=0, concat_axis=0, tiled=True)  22 us
    all_to_all x2, waiting for transfers between devices, sum_at_owner_2(): lax.all_to_all(blocks, axis, split_axis=0, concat_axis=0, tiled=True)  16.1 us
    all_to_all x1, starting transfers between devices, gather_over(): blocks = lax.all_to_all(blocks, axis, split_axis=0, concat_axis=0)  15.6 us
  transfers between devices with their start and end apart: 7, of which 7 were waited for; matrix products, arithmetic and copies ran while one was open for 5% of the time, Pallas kernels for 0%

profile of v1, /device:TPU:1, one launch (start us, length us, event | category | flops | bytes accessed | tf_op | source)
XLA Modules:
  0.0 272.5 jit_solution(3084040128954077170)
XLA Ops:
  4.2 15.6 %all-to-all-start = ((bf16[256,16,70]{2,1,0:T(8,128)(2,1)}), bf16[256,16,70]{2,1,0:T(8,128)(2,1)S(1)}, u32[]{:S(2)}, u32[]{:S(2)}) async-start(bf16[256,16,70]{2,1,0:T(8,128)(2,1)} %stack.2), calls=%async_computation | async-start | bytes 2097152 | tf_op jit(solution)/shard_map/all_to_all | solution.py:19
  19.8 2.8 %fusion.54 = (bf16[1,44,4096]{2,0,1:T(2,128)(2,1)}, bf16[1,44,4096]{2,0,1:T(2,128)(2,1)}) fusion(bf16[2,44,4096]{2,0,1:T(2,128)(2,1)S(1)} %copy-done.1), kind=kLoop, calls=%fused_computation.115 | loop fusion | bytes 1441792 | tf_op jit(solution)/shard_map/slice | solution.py:197
  22.6 2.8 %fusion.53 = (bf16[1,4096,44]{1,0,2:T(2,128)(2,1)}, bf16[1,4096,44]{1,0,2:T(2,128)(2,1)}) fusion(bf16[2,4096,44]{1,0,2:T(2,128)(2,1)S(1)} %copy-done.2), kind=kLoop, calls=%fused_computation.114 | loop fusion | bytes 1441792 | tf_op jit(solution)/shard_map/slice | solution.py:197
  28.0 22.4 %all-to-all-done = bf16[256,16,70]{2,1,0:T(8,128)(2,1)S(1)} async-done(((bf16[256,16,70]{2,1,0:T(8,128)(2,1)}), bf16[256,16,70]{2,1,0:T(8,128)(2,1)S(1)}, u32[]{:S(2)}, u32[]{:S(2)}) %all-to-all-start) | async-done | bytes 573472 | tf_op jit(solution)/shard_map/all_to_all | solution.py:19
  54.2 19.9 %all_to_all.81 = f32[8,32,1024]{2,1,0:T(8,128)S(1)} all-to-all(f32[8,32,1024]{2,1,0:T(8,128)S(1)} %bitcast.94), channel_id=1, replica_groups=mesh['kv_0'=8,'kv_1'=4,'tp_0'=4,'tp_1'=2] {'tp_0','tp_1'}, dimensions={0} | all-to-all | bytes 2097152 | tf_op jit(solution)/shard_map/all_to_all | solution.py:66
  74.4 12.5 %all_to_all.82 = f32[32,1,1024]{2,1,0:T(1,128)S(1)} all-to-all(f32[32,1,1024]{2,1,0:T(1,128)S(1)} %all_to_all.53), channel_id=1, replica_groups=mesh['kv_0'=8,'kv_1'=4,'tp_0'=4,'tp_1'=2] {'kv_0','kv_1'}, dimensions={0} | all-to-all | bytes 262144 | tf_op jit(solution)/shard_map/all_to_all | solution.py:74
  87.7 3.9 %all-to-all-start.3 = ((f32[32,1,1024]{2,1,0:T(1,128)}), f32[32,1,1024]{2,1,0:T(1,128)S(1)}, u32[]{:S(2)}, u32[]{:S(2)}) async-start(f32[32,1,1024]{2,1,0:T(1,128)} %broadcast_in_dim.12), calls=%async_computation.3 | async-start | bytes 262144 | tf_op jit(solution)/shard_map/all_to_all | solution.py:43
  91.9 9.1 %all-to-all-done.3 = f32[32,1,1024]{2,1,0:T(1,128)S(1)} async-done(((f32[32,1,1024]{2,1,0:T(1,128)}), f32[32,1,1024]{2,1,0:T(1,128)S(1)}, u32[]{:S(2)}, u32[]{:S(2)}) %all-to-all-start.3) | async-done | bytes 131104 | tf_op jit(solution)/shard_map/all_to_all | solution.py:43
  102.1 7.1 %all-to-all-start.4 = ((f32[8,32,1024]{2,1,0:T(8,128)}), f32[8,32,1024]{2,1,0:T(8,128)S(1)}, u32[]{:S(2)}, u32[]{:S(2)}) async-start(f32[8,32,1024]{2,1,0:T(8,128)} %broadcast_in_dim.13), calls=%async_computation.4 | async-start | bytes 2097152 | tf_op jit(solution)/shard_map/all_to_all | solution.py:43
  109.8 3.4 %convert_reduce_fusion = (f32[4096]{0:T(1024)S(1)}, f32[4096]{0:T(1024)S(1)}, f32[4096]{0:T(1024)S(1)}, f32[4096]{0:T(1024)S(1)}, f32[4096]{0:T(1024)S(1)}, /*index=5*/f32[4096]{0:T(1024)S(1)}) fusion(bf16[3,4096]{0,1:T(8,128)(2,1)S(1)} %get-tuple-element.17, bf16[3,4096]{0,1:T(8,128)(2,1)S(1)} %get-tuple-element.16), kind=kLoop, calls=%fused_computation.1 | loop fusion | flops 24576 | bytes 147456 | tf_op jit(solution)/shard_map/add | solution.py:100
  113.2 11.0 %all-to-all-done.4 = f32[8,32,1024]{2,1,0:T(8,128)S(1)} async-done(((f32[8,32,1024]{2,1,0:T(8,128)}), f32[8,32,1024]{2,1,0:T(8,128)S(1)}, u32[]{:S(2)}, u32[]{:S(2)}) %all-to-all-start.4) | async-done | bytes 1048608 | tf_op jit(solution)/shard_map/all_to_all | solution.py:43
  128.1 3.9 %all-to-all-start.5 = ((bf16[32,2,2048]{2,1,0:T(2,128)(2,1)}), bf16[32,2,2048]{2,1,0:T(2,128)(2,1)S(1)}, u32[]{:S(2)}, u32[]{:S(2)}) async-start(bf16[32,2,2048]{2,1,0:T(2,128)(2,1)} %pad_maximum_fusion), calls=%async_computation.5 | async-start | bytes 524288 | tf_op jit(solution)/shard_map/all_to_all | solution.py:87
  132.0 11.4 %all-to-all-done.5 = bf16[32,2,2048]{2,1,0:T(2,128)(2,1)S(1)} async-done(((bf16[32,2,2048]{2,1,0:T(2,128)(2,1)}), bf16[32,2,2048]{2,1,0:T(2,128)(2,1)S(1)}, u32[]{:S(2)}, u32[]{:S(2)}) %all-to-all-start.5) | async-done | bytes 262176 | tf_op jit(solution)/shard_map/all_to_all | solution.py:87
  145.6 3.5 %convolution_convert_fusion = bf16[2,4096]{1,0:T(2,128)(2,1)} fusion(bf16[512,4096]{1,0:T(8,128)(2,1)} %param.26, f32[1,2,4,128]{3,2,1,0:T(4,128)S(1)} %multiply_bitcast_fusion.2, bf16[2,2048]{1,0:T(2,128)(2,1)S(1)} %reduce_sum.124, f32[512]{0:T(512)S(1)} %copy-done.12), kind=kOutput, calls=%fused_computation | convolution fusion | flops 8404992 | bytes 4218880 | tf_op jit(solution)/shard_map/dot_general | solution.py:184
  149.0 5.9 %all-to-all-start.6 = ((bf16[8,2,512]{2,1,0:T(2,128)(2,1)}), bf16[8,2,512]{2,1,0:T(2,128)(2,1)S(1)}, u32[]{:S(2)}, u32[]{:S(2)}) async-start(bf16[8,2,512]{2,1,0:T(2,128)(2,1)} %bitcast.18), calls=%async_computation.6 | async-start | bytes 32768 | tf_op jit(solution)/shard_map/all_to_all | solution.py:87
  154.9 4.7 %all-to-all-done.6 = bf16[8,2,512]{2,1,0:T(2,128)(2,1)S(1)} async-done(((bf16[8,2,512]{2,1,0:T(2,128)(2,1)}), bf16[8,2,512]{2,1,0:T(2,128)(2,1)S(1)}, u32[]{:S(2)}, u32[]{:S(2)}) %all-to-all-start.6) | async-done | bytes 16416 | tf_op jit(solution)/shard_map/all_to_all | solution.py:87
  159.7 7.7 %all_to_all.83 = bf16[8,2,512]{2,1,0:T(2,128)(2,1)S(1)} all-to-all(bf16[8,2,512]{2,1,0:T(2,128)(2,1)S(1)} %broadcast_in_dim.14), channel_id=1, replica_groups=mesh['kv_0'=8,'kv_1'=4,'tp_0'=4,'tp_1'=2] {'tp_0','tp_1'}, dimensions={0} | all-to-all | bytes 32768 | tf_op jit(solution)/shard_map/all_to_all | solution.py:43
  167.9 19.6 %all_to_all.84 = bf16[32,2,4096]{2,1,0:T(2,128)(2,1)S(1)} all-to-all(bf16[32,2,4096]{2,1,0:T(2,128)(2,1)S(1)} %broadcast_in_dim.15), channel_id=1, replica_groups=mesh['kv_0'=8,'kv_1'=4,'tp_0'=4,'tp_1'=2] {'kv_0','kv_1'}, dimensions={0} | all-to-all | bytes 1048576 | tf_op jit(solution)/shard_map/all_to_all | solution.py:43
  193.7 19.7 %all_to_all.85 = f32[8,32,1024]{2,1,0:T(8,128)S(1)} all-to-all(f32[8,32,1024]{2,1,0:T(8,128)S(1)} %bitcast.95), channel_id=1, replica_groups=mesh['kv_0'=8,'kv_1'=4,'tp_0'=4,'tp_1'=2] {'tp_0','tp_1'}, dimensions={0} | all-to-all | bytes 2097152 | tf_op jit(solution)/shard_map/all_to_all | solution.py:66
  213.6 13.5 %all_to_all.86 = f32[32,1,1024]{2,1,0:T(1,128)S(1)} all-to-all(f32[32,1,1024]{2,1,0:T(1,128)S(1)} %all_to_all.63), channel_id=1, replica_groups=mesh['kv_0'=8,'kv_1'=4,'tp_0'=4,'tp_1'=2] {'kv_0','kv_1'}, dimensions={0} | all-to-all | bytes 262144 | tf_op jit(solution)/shard_map/all_to_all | solution.py:74
  228.0 3.9 %all-to-all-start.11 = ((f32[32,1,1024]{2,1,0:T(1,128)}), f32[32,1,1024]{2,1,0:T(1,128)S(1)}, u32[]{:S(2)}, u32[]{:S(2)}) async-start(f32[32,1,1024]{2,1,0:T(1,128)} %broadcast_in_dim.16), calls=%async_computation.11 | async-start | bytes 262144 | tf_op jit(solution)/shard_map/all_to_all | solution.py:43
  232.4 8.9 %all-to-all-done.11 = f32[32,1,1024]{2,1,0:T(1,128)S(1)} async-done(((f32[32,1,1024]{2,1,0:T(1,128)}), f32[32,1,1024]{2,1,0:T(1,128)S(1)}, u32[]{:S(2)}, u32[]{:S(2)}) %all-to-all-start.11) | async-done | bytes 131104 | tf_op jit(solution)/shard_map/all_to_all | solution.py:43
  242.4 7.1 %all-to-all-start.12 = ((f32[8,32,1024]{2,1,0:T(8,128)}), f32[8,32,1024]{2,1,0:T(8,128)S(1)}, u32[]{:S(2)}, u32[]{:S(2)}) async-start(f32[8,32,1024]{2,1,0:T(8,128)} %broadcast_in_dim.17), calls=%async_computation.12 | async-start | bytes 2097152 | tf_op jit(solution)/shard_map/all_to_all | solution.py:43
  250.8 13.8 %all-to-all-done.12 = f32[8,32,1024]{2,1,0:T(8,128)S(1)} async-done(((f32[8,32,1024]{2,1,0:T(8,128)}), f32[8,32,1024]{2,1,0:T(8,128)S(1)}, u32[]{:S(2)}, u32[]{:S(2)}) %all-to-all-start.12) | async-done | bytes 1048608 | tf_op jit(solution)/shard_map/all_to_all | solution.py:43
  (115 shorter events, 37.4 us)
Async XLA Ops:
  0.6 125.7 %copy-start = (bf16[128,512]{1,0:T(8,128)(2,1)S(1)}, bf16[128,512]{1,0:T(8,128)(2,1)}, u32[]{:S(2)}) copy-start(bf16[128,512]{1,0:T(8,128)(2,1)} %param.23) | copy-start | bytes 393220
  0.6 19.2 %copy-start.1 = (bf16[2,44,4096]{2,0,1:T(2,128)(2,1)S(1)}, bf16[2,44,4096]{2,0,1:T(2,128)(2,1)}, u32[]{:S(2)}) copy-start(bf16[2,44,4096]{2,0,1:T(2,128)(2,1)} %param.17) | copy-start | bytes 2162692
  4.2 18.5 %copy-start.2 = (bf16[2,4096,44]{1,0,2:T(2,128)(2,1)S(1)}, bf16[2,4096,44]{1,0,2:T(2,128)(2,1)}, u32[]{:S(2)}) copy-start(bf16[2,4096,44]{1,0,2:T(2,128)(2,1)} %param.16) | copy-start | bytes 2162692
  4.2 46.2 %all-to-all-start = ((bf16[256,16,70]{2,1,0:T(8,128)(2,1)}), bf16[256,16,70]{2,1,0:T(8,128)(2,1)S(1)}, u32[]{:S(2)}, u32[]{:S(2)}) async-start(bf16[256,16,70]{2,1,0:T(8,128)(2,1)} %stack.2), calls=%async_computation | async-start | bytes 2097152 | tf_op jit(solution)/shard_map/all_to_all | solution.py:19
  22.6 2.8 %copy-start.3 = (bf16[2,4096,44]{1,0,2:T(2,128)(2,1)S(1)}, bf16[2,4096,44]{1,0,2:T(2,128)(2,1)}, u32[]{:S(2)}) copy-start(bf16[2,4096,44]{1,0,2:T(2,128)(2,1)} %param.15) | copy-start | bytes 2162692
  87.7 13.3 %all-to-all-start.3 = ((f32[32,1,1024]{2,1,0:T(1,128)}), f32[32,1,1024]{2,1,0:T(1,128)S(1)}, u32[]{:S(2)}, u32[]{:S(2)}) async-start(f32[32,1,1024]{2,1,0:T(1,128)} %broadcast_in_dim.12), calls=%async_computation.3 | async-start | bytes 262144 | tf_op jit(solution)/shard_map/all_to_all | solution.py:43
  102.1 22.1 %all-to-all-start.4 = ((f32[8,32,1024]{2,1,0:T(8,128)}), f32[8,32,1024]{2,1,0:T(8,128)S(1)}, u32[]{:S(2)}, u32[]{:S(2)}) async-start(f32[8,32,1024]{2,1,0:T(8,128)} %broadcast_in_dim.13), calls=%async_computation.4 | async-start | bytes 2097152 | tf_op jit(solution)/shard_map/all_to_all | solution.py:43
  125.6 0.9 copy-start.8
  125.6 1.1 copy-start.9
  125.7 1.3 copy-start.10
  126.0 6.0 %copy-start.11 = (f32[512]{0:T(512)S(1)}, f32[512]{0:T(512)}, u32[]{:S(2)}) copy-start(f32[512]{0:T(512)} %param.24) | copy-start | bytes 6148
  126.0 17.7 %copy-start.7 = (f32[2,4,128,128]{3,2,1,0:T(8,128)S(1)}, f32[2,4,128,128]{3,2,1,0:T(8,128)}, u32[]{:S(2)}) copy-start(f32[2,4,128,128]{3,2,1,0:T(8,128)} %param.27) | copy-start | bytes 1572868
  126.5 19.1 %copy-start.12 = (f32[512]{0:T(512)S(1)}, f32[512]{0:T(512)}, u32[]{:S(2)}) copy-start(f32[512]{0:T(512)} %param.25) | copy-start | bytes 6148
  128.1 15.3 %all-to-all-start.5 = ((bf16[32,2,2048]{2,1,0:T(2,128)(2,1)}), bf16[32,2,2048]{2,1,0:T(2,128)(2,1)S(1)}, u32[]{:S(2)}, u32[]{:S(2)}) async-start(bf16[32,2,2048]{2,1,0:T(2,128)(2,1)} %pad_maximum_fusion), calls=%async_computation.5 | async-start | bytes 524288 | tf_op jit(solution)/shard_map/all_to_all | solution.py:87
  144.1 0.8 copy-start.4
  149.0 10.6 %all-to-all-start.6 = ((bf16[8,2,512]{2,1,0:T(2,128)(2,1)}), bf16[8,2,512]{2,1,0:T(2,128)(2,1)S(1)}, u32[]{:S(2)}, u32[]{:S(2)}) async-start(bf16[8,2,512]{2,1,0:T(2,128)(2,1)} %bitcast.18), calls=%async_computation.6 | async-start | bytes 32768 | tf_op jit(solution)/shard_map/all_to_all | solution.py:87
  167.9 22.1 %copy-start.6 = (bf16[1,4096,44]{1,0,2:T(2,128)(2,1)S(1)}, bf16[1,4096,44]{1,0,2:T(2,128)(2,1)}, u32[]{:S(2)}) copy-start(bf16[1,4096,44]{1,0,2:T(2,128)(2,1)} %get-tuple-element.18) | copy-start | bytes 1081348
  187.5 3.1 %copy-start.5 = (bf16[1,44,4096]{2,0,1:T(2,128)(2,1)S(1)}, bf16[1,44,4096]{2,0,1:T(2,128)(2,1)}, u32[]{:S(2)}) copy-start(bf16[1,44,4096]{2,0,1:T(2,128)(2,1)} %get-tuple-element.22) | copy-start | bytes 1081348
  228.0 13.3 %all-to-all-start.11 = ((f32[32,1,1024]{2,1,0:T(1,128)}), f32[32,1,1024]{2,1,0:T(1,128)S(1)}, u32[]{:S(2)}, u32[]{:S(2)}) async-start(f32[32,1,1024]{2,1,0:T(1,128)} %broadcast_in_dim.16), calls=%async_computation.11 | async-start | bytes 262144 | tf_op jit(solution)/shard_map/all_to_all | solution.py:43
  242.4 22.1 %all-to-all-start.12 = ((f32[8,32,1024]{2,1,0:T(8,128)}), f32[8,32,1024]{2,1,0:T(8,128)S(1)}, u32[]{:S(2)}, u32[]{:S(2)}) async-start(f32[8,32,1024]{2,1,0:T(8,128)} %broadcast_in_dim.17), calls=%async_computation.12 | async-start | bytes 2097152 | tf_op jit(solution)/shard_map/all_to_all | solution.py:43
